TPU v7x, 32 devices: a whole 2x2x4 slice. The times are simulated.
32 devices in a mesh: grp: 2 (over y), ep: 16 (over z, x, core), tp: 1.
Axes of the slice: x: 2, y: 2, z: 4, core: 2. Of those that a mesh axis runs over, the one named last changes fastest.
Arguments:
- tokens: bfloat16 [3072, 2048], P(('grp', 'ep')), parts along dimension 0, may hold values from -6 to 6
- prior_state: float32 [2, 3072, 4096], P(None, ('grp', 'ep'), 'tp'), parts along dimension 1, may hold values from -6 to 6
- mix_gain: float32 [2048], replicated, may hold values from 0.1 to 1.9
- in_weight: bfloat16 [2048, 1024], P(None, 'tp'), may hold values from -0.125 to 0.125
- decay_rate: float32 [64, 64], P('tp'), may hold values from 0.2 to 20
- frequency: float32 [64, 64], P('tp'), may hold values from 0 to 12
- log_step: float32 [64], P('tp'), may hold values from -4.6 to 0
- input_map: float32 [2, 64, 64, 16], P(None, 'tp'), may hold values from -6 to 6
- output_map: float32 [2, 64, 16, 64], P(None, 'tp'), may hold values from -0.5 to 0.5
- skip_gain: float32 [1024], P('tp'), may hold values from -4 to 4
- out_weight: bfloat16 [1024, 2048], P('tp'), may hold values from -0.1875 to 0.1875
- channel_gain: float32 [2048], replicated, may hold values from 0.1 to 1.9
- expert_gate: bfloat16 [16, 2048, 512], P('ep', None, 'tp'), may hold values from -0.125 to 0.125
- expert_up: bfloat16 [16, 2048, 512], P('ep', None, 'tp'), may hold values from -0.125 to 0.125
- expert_down: bfloat16 [16, 512, 2048], P('ep', 'tp'), may hold values from -0.25 to 0.25
- shared_gate: bfloat16 [2048, 512], P(None, 'tp'), may hold values from -0.125 to 0.125
- shared_up: bfloat16 [2048, 512], P(None, 'tp'), may hold values from -0.125 to 0.125
- shared_down: bfloat16 [512, 2048], P('tp'), may hold values from -0.25 to 0.25
- routes: int32 [3072, 6], P(('grp', 'ep')), parts along dimension 0, may hold values from 0 to 15, all different within a row; in each aligned block of 96 rows (0 to 95, 96 to 191, ...) at most 54 rows name the same one
- route_weights: float32 [3072, 6], P(('grp', 'ep')), parts along dimension 0, may hold values from 0.05 to 0.8
Outputs:
- layer_out: bfloat16 [3072, 2048], P(('grp', 'ep'), 'tp'), parts along dimension 0
- new_state: float32 [2, 3072, 4096], P(None, ('grp', 'ep'), 'tp'), parts along dimension 1
There are 2 independent parts, one for each index of `grp`. A program takes and returns all parts, laid end to end along the dimension named above; an argument that names none is the same for every part. Nothing has to cross between parts.
Inputs may be any that keep to these rules, and one draw needn't show every extreme that they name: `routes`: each row names 6 different experts; among the rows of one index of ep no expert is named by more than 54 rows.
All inputs are finite; a program needn't handle non-finite values.
Results may differ from a plain program's by a relative error of at most 0.017.
Values may be sent and summed in bfloat16 or wider, within the bound.
A program may use at most 128 MiB of HBM per device.

v0:
```python
import jax
import jax.numpy as jnp
from jax import lax
from jax.sharding import PartitionSpec as P

norm_eps = 1e-06
highest = lax.Precision.HIGHEST


def root_scale(activations, scale_gain):
    values = activations.astype(jnp.float32)
    factor = lax.rsqrt(jnp.mean(values * values, axis=-1, keepdims=True) + norm_eps)
    return (values * factor * scale_gain).astype(jnp.bfloat16)


def state_update(
    drive_rows, prior_state, decay_rate, frequency, log_step, input_map, output_map, skip_gain
):
    sequences = drive_rows.shape[0]
    groups = decay_rate.shape[0]
    driven = drive_rows.astype(jnp.float32).reshape(sequences, groups, -1)
    step_size = jnp.exp(log_step)[:, None]
    real_rate = -decay_rate
    magnitude = jnp.exp(real_rate * step_size)
    turn_real = magnitude * jnp.cos(frequency * step_size)
    turn_imag = magnitude * jnp.sin(frequency * step_size)
    denominator = real_rate * real_rate + frequency * frequency
    hold_real = ((turn_real - 1.0) * real_rate + turn_imag * frequency) / denominator
    hold_imag = (turn_imag * real_rate - (turn_real - 1.0) * frequency) / denominator
    push_real = jnp.einsum("sgh,gph->sgp", driven, input_map[0], precision=highest)
    push_imag = jnp.einsum("sgh,gph->sgp", driven, input_map[1], precision=highest)
    enter_real = push_real * hold_real - push_imag * hold_imag
    enter_imag = push_real * hold_imag + push_imag * hold_real
    old_real = prior_state[0].reshape(sequences, groups, -1)
    old_imag = prior_state[1].reshape(sequences, groups, -1)
    fresh_real = turn_real * old_real - turn_imag * old_imag + enter_real
    fresh_imag = turn_real * old_imag + turn_imag * old_real + enter_imag
    readout = jnp.einsum("ghp,sgp->sgh", output_map[0], fresh_real, precision=highest)
    readout = readout - jnp.einsum("ghp,sgp->sgh", output_map[1], fresh_imag, precision=highest)
    readout = readout.reshape(sequences, -1) + skip_gain * drive_rows.astype(jnp.float32)
    fresh = jnp.stack([fresh_real.reshape(sequences, -1), fresh_imag.reshape(sequences, -1)])
    return (readout, fresh)


def exchanged_experts(second_normed, routes, route_weights, expert_gate, expert_up, expert_down):
    experts = lax.axis_size("ep")
    seq_rows, top_count = routes.shape
    slot_cap = min(seq_rows, max(2, 3 * seq_rows * top_count // (2 * experts)))
    flat_routes = routes.reshape(-1)
    one_hot = (flat_routes[:, None] == jnp.arange(experts, dtype=jnp.int32)[None, :]).astype(
        jnp.int32
    )
    ranked = jnp.sum((jnp.cumsum(one_hot, axis=0) - one_hot) * one_hot, axis=1)
    slot_index = flat_routes * slot_cap + ranked
    placed = slot_index[:, None] == jnp.arange(experts * slot_cap, dtype=jnp.int32)[None, :]
    placed_rows = jnp.any(placed.reshape(seq_rows, top_count, experts * slot_cap), axis=1).astype(
        jnp.bfloat16
    )
    outgoing = lax.dot_general(
        placed_rows, second_normed, (((0,), (0,)), ((), ())), preferred_element_type=jnp.float32
    ).astype(jnp.bfloat16)
    outgoing = outgoing.reshape(experts, slot_cap, -1)
    arrived = lax.all_to_all(outgoing, "ep", split_axis=0, concat_axis=0, tiled=True)
    sources, count_items, full_width = arrived.shape
    expert_rows = arrived.reshape(sources * count_items, full_width)
    gate_val = jnp.dot(expert_rows, expert_gate[0], preferred_element_type=jnp.float32)
    up_val = jnp.dot(expert_rows, expert_up[0], preferred_element_type=jnp.float32)
    hidden = (jax.nn.silu(gate_val) * up_val).astype(jnp.bfloat16)
    piece = jnp.dot(hidden, expert_down[0], preferred_element_type=jnp.float32)
    summed = lax.psum_scatter(
        piece.reshape(sources, count_items, full_width).astype(jnp.bfloat16),
        "tp",
        scatter_dimension=2,
        tiled=True,
    )
    returned = lax.all_to_all(summed, "ep", split_axis=0, concat_axis=0, tiled=True)
    flat_back = returned.reshape(experts * slot_cap, -1)
    picked = (
        jnp.take(flat_back, slot_index, axis=0).reshape(seq_rows, top_count, -1).astype(jnp.float32)
    )
    routed = jnp.einsum("sk,skd->sd", route_weights, picked)
    return routed


def gathered_experts(second_normed, routes, route_weights, expert_gate, expert_up, expert_down):
    all_routes = lax.all_gather(routes, "ep", axis=0, tiled=True)
    all_weights = lax.all_gather(route_weights, "ep", axis=0, tiled=True)
    here = all_routes == lax.axis_index("ep")
    weight = jnp.sum(jnp.where(here, all_weights, 0.0), axis=1)
    rows = lax.all_gather(second_normed, "ep", axis=0, tiled=True)
    gate_val = jnp.dot(rows, expert_gate[0], preferred_element_type=jnp.float32)
    up_val = jnp.dot(rows, expert_up[0], preferred_element_type=jnp.float32)
    hidden = (jax.nn.silu(gate_val) * up_val).astype(jnp.bfloat16)
    piece = jnp.dot(hidden, expert_down[0], preferred_element_type=jnp.float32)
    summed = lax.psum_scatter(piece.astype(jnp.bfloat16), "tp", scatter_dimension=1, tiled=True)
    weighted = (weight[:, None] * summed.astype(jnp.float32)).astype(jnp.bfloat16)
    return lax.psum_scatter(weighted, "ep", scatter_dimension=0, tiled=True).astype(jnp.float32)


def body(
    tokens,
    prior_state,
    mix_gain,
    in_weight,
    decay_rate,
    frequency,
    log_step,
    input_map,
    output_map,
    skip_gain,
    out_weight,
    channel_gain,
    expert_gate,
    expert_up,
    expert_down,
    shared_gate,
    shared_up,
    shared_down,
    routes,
    route_weights,
):
    normed = root_scale(tokens, mix_gain)
    drive_rows = jnp.dot(normed, in_weight, preferred_element_type=jnp.float32).astype(jnp.bfloat16)
    readout, new_state = state_update(
        drive_rows, prior_state, decay_rate, frequency, log_step, input_map, output_map, skip_gain
    )
    activated = jax.nn.gelu(readout).astype(jnp.bfloat16)
    partial_value = jnp.dot(activated, out_weight, preferred_element_type=jnp.float32)
    mixer_out = lax.psum(partial_value.astype(jnp.bfloat16), "tp").astype(jnp.float32)
    middle = (tokens.astype(jnp.float32) + mixer_out).astype(jnp.bfloat16)
    second_normed = root_scale(middle, channel_gain)
    shared_gval = jnp.dot(second_normed, shared_gate, preferred_element_type=jnp.float32)
    shared_uval = jnp.dot(second_normed, shared_up, preferred_element_type=jnp.float32)
    shared_hidden = (jax.nn.silu(shared_gval) * shared_uval).astype(jnp.bfloat16)
    shared_piece = jnp.dot(shared_hidden, shared_down, preferred_element_type=jnp.float32)
    shared_out = lax.psum_scatter(
        shared_piece.astype(jnp.bfloat16), "tp", scatter_dimension=1, tiled=True
    ).astype(jnp.float32)
    experts = lax.axis_size("ep")
    half_cols = second_normed.shape[1] // lax.axis_size("tp")
    if experts <= 16:
        routed = gathered_experts(
            second_normed, routes, route_weights, expert_gate, expert_up, expert_down
        )
    else:
        routed = exchanged_experts(
            second_normed, routes, route_weights, expert_gate, expert_up, expert_down
        )
    own_middle = lax.dynamic_slice_in_dim(middle, lax.axis_index("tp") * half_cols, half_cols, 1)
    layer_out = (own_middle.astype(jnp.float32) + routed + shared_out).astype(jnp.bfloat16)
    return (layer_out, new_state)


def solution(mesh):
    in_specs = (
        P(("grp", "ep"), None),
        P(None, ("grp", "ep"), "tp"),
        P(),
        P(None, "tp"),
        P("tp", None),
        P("tp", None),
        P("tp"),
        P(None, "tp", None, None),
        P(None, "tp", None, None),
        P("tp"),
        P("tp", None),
        P(),
        P("ep", None, "tp"),
        P("ep", None, "tp"),
        P("ep", "tp", None),
        P(None, "tp"),
        P(None, "tp"),
        P("tp", None),
        P(("grp", "ep"), None),
        P(("grp", "ep"), None),
    )
    out_specs = (P(("grp", "ep"), "tp"), P(None, ("grp", "ep"), "tp"))
    return jax.shard_map(body, mesh=mesh, in_specs=in_specs, out_specs=out_specs, check_vma=False)
```

profile of v0, /device:TPU:0, one launch (start us, length us, event | category | flops | bytes accessed | tf_op | source)
XLA Modules:
  0.0 219.6 jit_solution(10515037456347401280)
XLA Ops:
  7.2 0.8 exp.14
  8.0 1.2 fusion.13
  9.2 3.2 %convolution_convert_fusion.3 = bf16[96,1024]{1,0:T(8,128)(2,1)S(1)} fusion(bf16[2048,1024]{1,0:T(8,128)(2,1)} %param.23, bf16[96,2048]{1,0:T(8,128)(2,1)} %param.20, f32[2048]{0:T(1024)} %param.22, f32[96]{0:T(128)S(1)} %add_rsqrt_fusion.1), kind=kOutput, calls=%fused_computation.23 | convolution fusion | flops 403537920 | bytes 4792704 | tf_op jit(solution)/shard_map/dot_general | solution.py:123
  12.6 3.8 %fusion.58 = (f32[1,96,4096]{2,1,0:T(8,128)}, f32[1,96,4096]{2,1,0:T(8,128)}) fusion(f32[2,96,4096]{2,1,0:T(8,128)} %param.21), kind=kLoop, calls=%fused_computation.79 | loop fusion | bytes 6291456 | tf_op jit(solution)/shard_map/slice | solution.py:34
  16.4 2.8 %copy.35 = f32[1,96,4096]{1,2,0:T(8,128)} copy(f32[1,96,4096]{2,1,0:T(8,128)} %get-tuple-element.4) | data formatting | bytes 3145728 | tf_op jit(solution)/shard_map/slice | solution.py:34
  19.2 2.8 %copy.36 = f32[1,96,4096]{1,2,0:T(8,128)} copy(f32[1,96,4096]{2,1,0:T(8,128)} %get-tuple-element.5) | data formatting | bytes 3145728 | tf_op jit(solution)/shard_map/slice | solution.py:35
  22.0 3.0 %fusion.23 = f32[64,96,64]{1,2,0:T(8,128)S(1)} fusion(bf16[96,64,16]{0,2,1:T(8,128)(2,1)S(1)} %bitcast.56, f32[2,64,64,16]{2,3,1,0:T(8,128)} %param.27), kind=kOutput, calls=%fused_computation.37 | convolution fusion | flops 75497472 | bytes 2293760 | tf_op jit(solution)/shard_map/sgh,gph->sgp/dot_general | solution.py:30
  25.3 5.7 %bitcast_add_fusion = (f32[96,64,64]{0,2,1:T(8,128)S(1)}, f32[96,64,64]{0,2,1:T(8,128)S(1)}) fusion(f32[64,96,64]{1,2,0:T(8,128)S(1)} %fusion.23, f32[96,64,64]{0,2,1:T(8,128)S(1)} %bitcast.54, f32[96,64,64]{0,2,1:T(8,128)} %bitcast.55, f32[64,64]{1,0:T(8,128)S(1)} %get-tuple-element.8, f32[64,64]{1,0:T(8,128)S(1)} %get-tuple-element.7, ...), kind=kOutput, calls=%fused_computation.18 | convolution fusion | flops 81002496 | bytes 9175040 | tf_op jit(solution)/shard_map/sgh,gph->sgp/dot_general | solution.py:31
  31.1 1.9 fusion.19
  33.0 1.9 convolution_subtract_fusion
  34.9 0.9 copy.38
  35.9 3.3 %multiply_reduce_fusion = (f32[96]{0:T(128)S(1)}, f32[96,2048]{1,0:T(8,128)S(1)}) fusion(bf16[1024,2048]{1,0:T(8,128)(2,1)} %param.30, f32[96,1024]{1,0:T(8,128)} %copy.38, bf16[96,1024]{1,0:T(8,128)(2,1)S(1)} %convolution_convert_fusion.3, f32[1024]{0:T(1024)S(1)} %copy-done.13, bf16[96,2048]{1,0:T(8,128)(2,1)S(1)} %copy-done.6), kind=kOutput, calls=%fused_computation.30 | convolution fusion | flops 405405600 | bytes 5968256 | tf_op jit(solution)/shard_map/dot_general | solution.py:128
  39.2 0.9 multiply_convert_fusion.1
  40.2 23.8 %all-gather = s32[16,96,6]{1,2,0:T(8,128)S(1)} all-gather(s32[1,96,6]{1,2,0:T(8,128)S(1)} %bitcast.59), channel_id=1, replica_groups=mesh['grp'=2,'ep'=16,'tp'=1] {'ep'}, dimensions={0}, use_global_device_ids=true | all-gather | bytes 39168 | tf_op jit(solution)/shard_map/all_gather | solution.py:86
  64.0 18.2 %all-gather.1 = f32[16,96,6]{1,2,0:T(8,128)S(1)} all-gather(f32[1,96,6]{1,2,0:T(8,128)S(1)} %bitcast.60), channel_id=1, replica_groups=mesh['grp'=2,'ep'=16,'tp'=1] {'ep'}, dimensions={0}, use_global_device_ids=true | all-gather | bytes 39168 | tf_op jit(solution)/shard_map/all_gather | solution.py:87
  82.3 22.4 %all-gather.4.cloned.1.call-done = bf16[1536,2048]{1,0:T(8,128)(2,1)} async-done(((bf16[96,2048]{1,0:T(8,128)(2,1)}), bf16[1536,2048]{1,0:T(8,128)(2,1)}) %all-gather.4.cloned.1.call-update) | async-done | bytes 6291472 | tf_op jit(solution)/shard_map/all_gather | solution.py:90
  104.7 8.5 %fusion.10 = f32[1536,512]{1,0:T(8,128)} fusion(bf16[1536,2048]{1,0:T(8,128)(2,1)} %all-gather.4.cloned.1.call-done, bf16[1,2048,512]{2,1,0:T(8,128)(2,1)} %param.32), kind=kOutput, calls=%fused_computation.16 | convolution fusion | flops 3221225472 | bytes 11534336 | tf_op jit(solution)/shard_map/dot_general | solution.py:91
  113.2 11.8 %multiply_convert_fusion = bf16[1536,2048]{1,0:T(8,128)(2,1)} fusion(f32[1536]{0:T(1024)S(1)} %reshape.45, bf16[1,512,2048]{2,1,0:T(8,128)(2,1)S(1)} %copy-done, bf16[1536,2048]{1,0:T(8,128)(2,1)} %all-gather.4.cloned.1.call-done, f32[1536,512]{1,0:T(8,128)} %fusion.10, bf16[1,2048,512]{2,1,0:T(8,128)(2,1)} %param.33), kind=kOutput, calls=%fused_computation | convolution fusion | flops 6459752448 | bytes 19929088 | tf_op jit(solution)/shard_map/dot_general | solution.py:94
  125.0 2.8 %copy.39 = f32[1,96,4096]{2,1,0:T(8,128)} copy(f32[1,96,4096]{1,2,0:T(8,128)} %bitcast.53) | data formatting | bytes 3145728 | tf_op jit(solution)/shard_map/stack;reshape | solution.py:41
  127.8 2.9 %copy.40 = f32[1,96,4096]{2,1,0:T(8,128)} copy(f32[1,96,4096]{1,2,0:T(8,128)} %bitcast.52) | data formatting | bytes 3145728 | tf_op jit(solution)/shard_map/stack;reshape | solution.py:41
  130.7 2.4 %fusion.59 = f32[96,512]{1,0:T(8,128)S(1)} fusion(bf16[96,2048]{1,0:T(8,128)(2,1)S(1)} %copy-done.5, bf16[2048,512]{1,0:T(8,128)(2,1)} %param.35), kind=kOutput, calls=%fused_computation.80 | convolution fusion | flops 201326592 | bytes 2686976 | tf_op jit(solution)/shard_map/dot_general | solution.py:132
  133.1 3.4 %pad_maximum_fusion = f32[2,96,4096]{2,1,0:T(8,128)} fusion(f32[1,96,4096]{2,1,0:T(8,128)} %copy.40, f32[1,96,4096]{2,1,0:T(8,128)S(1)} %copy-done.4), kind=kLoop, calls=%fused_computation.3 | loop fusion | flops 786432 | bytes 6291456 | tf_op jit(solution)/shard_map/stack | solution.py:41
  136.5 72.4 %reduce-scatter.2.cloned.1.call-done = bf16[96,2048]{1,0:T(8,128)(2,1)} async-done(((bf16[1536,2048]{1,0:T(8,128)(2,1)}), bf16[96,2048]{1,0:T(8,128)(2,1)}) %reduce-scatter.2.cloned.1.call-update) | async-done | bytes 393232 | tf_op jit(solution)/shard_map/reduce_scatter | solution.py:97
  208.9 3.9 %fusion.3 = bf16[96,2048]{1,0:T(8,128)(2,1)} fusion(bf16[512,2048]{1,0:T(8,128)(2,1)} %param.37, bf16[96,2048]{1,0:T(8,128)(2,1)S(1)} %copy-done.5, bf16[2048,512]{1,0:T(8,128)(2,1)} %param.36, f32[96,2048]{1,0:T(8,128)S(1)} %get-tuple-element.11, bf16[96,2048]{1,0:T(8,128)(2,1)} %reduce-scatter.2.cloned.1.call-done, f32[96,512]{1,0:T(8,128)S(1)} %fusion.59), kind=kOutput, calls=%fused_computation.8 | convolution fusion | flops 404127744 | bytes 6356992 | tf_op jit(solution)/shard_map/dot_general | solution.py:135
  (38 shorter events, 0.7 us)
Async XLA Ops:
  7.2 106.0 %copy-start = (bf16[1,512,2048]{2,1,0:T(8,128)(2,1)S(1)}, bf16[1,512,2048]{2,1,0:T(8,128)(2,1)}, u32[]{:S(2)}) copy-start(bf16[1,512,2048]{2,1,0:T(8,128)(2,1)} %param.34) | copy-start | bytes 6291460
  7.2 97.5 %all-gather.4.cloned.1.call-start = ((), (), s32[]{:S(2)}) async-start(), calls=%async_computation.1 | async-start | bytes 6684672 | tf_op jit(solution)/shard_map/all_gather | solution.py:90
  22.0 3.0 %copy-start.8 = (f32[64,64]{1,0:T(8,128)S(1)}, f32[64,64]{1,0:T(8,128)}, u32[]{:S(2)}) copy-start(f32[64,64]{1,0:T(8,128)} %param.25) | copy-start | bytes 49156
  22.0 3.0 %copy-start.9 = (f32[64,64]{1,0:T(8,128)S(1)}, f32[64,64]{1,0:T(8,128)}, u32[]{:S(2)}) copy-start(f32[64,64]{1,0:T(8,128)} %param.24) | copy-start | bytes 49156
  22.0 3.3 %copy-start.3 = (f32[1,96,4096]{1,2,0:T(8,128)S(1)}, f32[1,96,4096]{1,2,0:T(8,128)}, u32[]{:S(2)}) copy-start(f32[1,96,4096]{1,2,0:T(8,128)} %copy.35) | copy-start | bytes 4718596
  25.3 5.7 %copy-start.7 = (f32[2,64,16,64]{3,2,1,0:T(8,128)S(1)}, f32[2,64,16,64]{3,2,1,0:T(8,128)}, u32[]{:S(2)}) copy-start(f32[2,64,16,64]{3,2,1,0:T(8,128)} %param.28) | copy-start | bytes 1572868
  31.0 3.9 %copy-start.1 = (f32[96,64,64]{0,2,1:T(8,128)}, f32[96,64,64]{0,2,1:T(8,128)S(1)}, u32[]{:S(2)}) copy-start(f32[96,64,64]{0,2,1:T(8,128)S(1)} %get-tuple-element.2) | copy-start | bytes 4718596
  31.0 3.9 %copy-start.2 = (f32[96,64,64]{0,2,1:T(8,128)}, f32[96,64,64]{0,2,1:T(8,128)S(1)}, u32[]{:S(2)}) copy-start(f32[96,64,64]{0,2,1:T(8,128)S(1)} %get-tuple-element.3) | copy-start | bytes 4718596
  33.0 2.9 %copy-start.6 = (bf16[96,2048]{1,0:T(8,128)(2,1)S(1)}, bf16[96,2048]{1,0:T(8,128)(2,1)}, u32[]{:S(2)}) copy-start(bf16[96,2048]{1,0:T(8,128)(2,1)} %param.20) | copy-start | bytes 1179652
  33.0 2.9 %copy-start.13 = (f32[1024]{0:T(1024)S(1)}, f32[1024]{0:T(1024)}, u32[]{:S(2)}) copy-start(f32[1024]{0:T(1024)} %param.29) | copy-start | bytes 12292
  35.9 3.4 %copy-start.10 = (f32[2048]{0:T(1024)S(1)}, f32[2048]{0:T(1024)}, u32[]{:S(2)}) copy-start(f32[2048]{0:T(1024)} %param.31) | copy-start | bytes 24580
  35.9 4.3 %copy-start.11 = (s32[96,6]{0,1:T(8,128)S(1)}, s32[96,6]{0,1:T(8,128)}, u32[]{:S(2)}) copy-start(s32[96,6]{0,1:T(8,128)} %param.38) | copy-start | bytes 6916
  35.9 28.1 %copy-start.12 = (f32[96,6]{0,1:T(8,128)S(1)}, f32[96,6]{0,1:T(8,128)}, u32[]{:S(2)}) copy-start(f32[96,6]{0,1:T(8,128)} %param.39) | copy-start | bytes 6916
  40.2 168.7 %reduce-scatter.2.cloned.1.call-start = ((), (), s32[]{:S(2)}) async-start(), calls=%async_computation.2 | async-start | bytes 6684672 | tf_op jit(solution)/shard_map/reduce_scatter | solution.py:97
  127.8 2.9 %copy-start.5 = (bf16[96,2048]{1,0:T(8,128)(2,1)S(1)}, bf16[96,2048]{1,0:T(8,128)(2,1)}, u32[]{:S(2)}) copy-start(bf16[96,2048]{1,0:T(8,128)(2,1)} %multiply_convert_fusion.1) | copy-start | bytes 1179652
  130.7 2.4 %copy-start.4 = (f32[1,96,4096]{2,1,0:T(8,128)S(1)}, f32[1,96,4096]{2,1,0:T(8,128)}, u32[]{:S(2)}) copy-start(f32[1,96,4096]{2,1,0:T(8,128)} %copy.39) | copy-start | bytes 4718596
Sparse Core Ops, SparseCore 0:
  40.3 64.3 all-gather.3
  125.1 83.7 reduce-scatter.1
where the time goes:
time: 220 us
  waiting for transfers between devices  94.8 us (43%)
  matrix products  45.6 us (21%)
  blocking collectives  42 us (19%)
  local copies, waits for them, and re-layouts  17.2 us (8%)
  between operations  14.2 us (6%)
  other arithmetic  5.75 us (3%)
    reduce_scatter x1, waiting for transfers between devices, gathered_experts(): lax.psum_scatter(weighted, 'ep', scatter_dimension=0, tiled=True)  72.4 us
    all_gather x1, blocking collectives, gathered_experts(): all_routes = lax.all_gather(routes, 'ep', axis=0, tiled=True)  23.8 us
    all_gather x1, waiting for transfers between devices, gathered_experts(): rows = lax.all_gather(second_normed, 'ep', axis=0, tiled=True)  22.4 us
    all_gather x1, blocking collectives, gathered_experts(): all_weights = lax.all_gather(route_weights, 'ep', axis=0, tiled=True)  18.2 us
    dot_general x1, matrix products, gathered_experts(): piece = jnp.dot(hidden, expert_down[0], preferred_element_type=jnp.float32)  11.8 us
    dot_general x1, matrix products, gathered_experts(): gate_val = jnp.dot(rows, expert_gate[0], preferred_element_type=jnp.float32)  8.51 us
    slice x2, local copies, waits for them, and re-layouts, state_update(): old_real = prior_state[0].reshape(sequences, groups, -1)  6.61 us
    another operation x2, local copies, waits for them, and re-layouts, state_update(): jnp.stack([fresh_real.reshape(sequences, -1), fresh_imag.reshape(sequence...  5.71 us
  transfers between devices with their start and end apart: 2, of which 2 were waited for; matrix products, arithmetic and copies ran while one was open for 5% of the time, Pallas kernels for 0%

commit v1 on v0

--- a/solution.py
+++ b/solution.py
@@ -84,7 +84,14 @@
 
 def gathered_experts(second_normed, routes, route_weights, expert_gate, expert_up, expert_down):
     all_routes = lax.all_gather(routes, "ep", axis=0, tiled=True)
-    all_weights = lax.all_gather(route_weights, "ep", axis=0, tiled=True)
+    size = lax.axis_size("ep")
+    right = [(i, (i + 1) % size) for i in range(size)]
+    parts = [route_weights]
+    for reach in range(1, size):
+        parts = [lax.ppermute(parts[0], "ep", right), *parts]
+    whole = jnp.concatenate(parts, axis=0)
+    turn = (lax.axis_index("ep") + 1) * parts[-1].shape[0]
+    all_weights = jnp.roll(whole, turn, axis=0)
     here = all_routes == lax.axis_index("ep")
     weight = jnp.sum(jnp.where(here, all_weights, 0.0), axis=1)
     rows = lax.all_gather(second_normed, "ep", axis=0, tiled=True)

time: 220 us -> 256 us (1.16)
  waiting for transfers between devices: 94.8 us -> 153 us
  blocking collectives: 42 us -> 18.1 us
    ppermute x0 -> x15, waiting for transfers between devices: none -> 81.6 us  [gathered_experts(): parts = [lax.ppermute(parts[0], 'ep', right), *parts]]
    all_gather x1, waiting for transfers between devices: 22.4 us -> 0.02 us  [gathered_experts(): rows = lax.all_gather(second_normed, 'ep', axis=0, tiled=True)]
    all_gather x1 -> x0, blocking collectives: 18.2 us -> none  [gathered_experts(): all_weights = lax.all_gather(route_weights, 'ep', axis=0, tiled=True)]
    all_gather x1, blocking collectives: 23.8 us -> 18.1 us  [gathered_experts(): all_routes = lax.all_gather(routes, 'ep', axis=0, tiled=True)]
  transfers between devices with their start and end apart: 2 -> 17, of which waited for: 2 -> 15; matrix products, arithmetic and copies ran while one was open for 5% -> 5% of each run, Pallas kernels for 0% -> 0%
where the time goes in v1:
time: 256 us; the launch traced here: 255 us
  waiting for transfers between devices  153 us (60%)
  matrix products  45.6 us (18%)
  blocking collectives  18.1 us (7%)
  local copies, waits for them, and re-layouts  17.3 us (7%)
  between operations  14.3 us (6%)
  other arithmetic  5.84 us (2%)
    ppermute x15, waiting for transfers between devices, gathered_experts(): parts = [lax.ppermute(parts[0], 'ep', right), *parts]  81.6 us
    reduce_scatter x1, waiting for transfers between devices, gathered_experts(): lax.psum_scatter(weighted, 'ep', scatter_dimension=0, tiled=True)  71.8 us
    all_gather x1, blocking collectives, gathered_experts(): all_routes = lax.all_gather(routes, 'ep', axis=0, tiled=True)  18.1 us
    dot_general x1, matrix products, gathered_experts(): piece = jnp.dot(hidden, expert_down[0], preferred_element_type=jnp.float32)  11.8 us
    dot_general x1, matrix products, gathered_experts(): gate_val = jnp.dot(rows, expert_gate[0], preferred_element_type=jnp.float32)  8.52 us
    slice x2, local copies, waits for them, and re-layouts, state_update(): old_real = prior_state[0].reshape(sequences, groups, -1)  6.59 us
    another operation x2, local copies, waits for them, and re-layouts, state_update(): jnp.stack([fresh_real.reshape(sequences, -1), fresh_imag.reshape(sequence...  5.73 us
    dot_general x1, matrix products, state_update(): jnp.einsum('sgh,gph->sgp', driven, input_map[1], precision=highest)  5.71 us
  transfers between devices with their start and end apart: 17, of which 15 were waited for; matrix products, arithmetic and copies ran while one was open for 5% of the time, Pallas kernels for 0%

profile of v1, /device:TPU:0, one launch (start us, length us, event | category | flops | bytes accessed | tf_op | source)
XLA Modules:
  0.0 255.4 jit_solution(12569279599424782163)
XLA Ops:
  9.2 3.2 %convolution_convert_fusion.3 = bf16[96,1024]{1,0:T(8,128)(2,1)S(1)} fusion(bf16[2048,1024]{1,0:T(8,128)(2,1)} %param.23, bf16[96,2048]{1,0:T(8,128)(2,1)} %param.20, f32[2048]{0:T(1024)} %param.22, f32[96]{0:T(128)S(1)} %add_rsqrt_fusion.1), kind=kOutput, calls=%fused_computation.23 | convolution fusion | flops 403537920 | bytes 4792704 | tf_op jit(solution)/shard_map/dot_general | solution.py:130
  12.6 3.8 %fusion.60 = (f32[1,96,4096]{2,1,0:T(8,128)}, f32[1,96,4096]{2,1,0:T(8,128)}) fusion(f32[2,96,4096]{2,1,0:T(8,128)} %param.21), kind=kLoop, calls=%fused_computation.80 | loop fusion | bytes 6291456 | tf_op jit(solution)/shard_map/slice | solution.py:34
  25.3 5.7 %bitcast_add_fusion = (f32[96,64,64]{0,2,1:T(8,128)S(1)}, f32[96,64,64]{0,2,1:T(8,128)S(1)}) fusion(f32[64,96,64]{1,2,0:T(8,128)S(1)} %fusion.25, f32[96,64,64]{0,2,1:T(8,128)S(1)} %bitcast.57, f32[96,64,64]{0,2,1:T(8,128)} %bitcast.58, f32[64,64]{1,0:T(8,128)S(1)} %get-tuple-element.8, f32[64,64]{1,0:T(8,128)S(1)} %get-tuple-element.7, ...), kind=kOutput, calls=%fused_computation.18 | convolution fusion | flops 81002496 | bytes 9175040 | tf_op jit(solution)/shard_map/sgh,gph->sgp/dot_general | solution.py:31
  35.9 3.3 %multiply_reduce_fusion = (f32[96]{0:T(128)S(1)}, f32[96,2048]{1,0:T(8,128)S(1)}) fusion(bf16[1024,2048]{1,0:T(8,128)(2,1)} %param.30, f32[96,1024]{1,0:T(8,128)} %copy.53, bf16[96,1024]{1,0:T(8,128)(2,1)S(1)} %convolution_convert_fusion.3, f32[1024]{0:T(1024)S(1)} %copy-done.13, bf16[96,2048]{1,0:T(8,128)(2,1)S(1)} %copy-done.6), kind=kOutput, calls=%fused_computation.30 | convolution fusion | flops 405405600 | bytes 5968256 | tf_op jit(solution)/shard_map/dot_general | solution.py:135
  40.7 6.2 %collective-permute-done = f32[96,6]{0,1:T(8,128)S(1)} collective-permute-done((f32[96,6]{0,1:T(8,128)S(1)}, f32[96,6]{0,1:T(8,128)S(1)}, u32[]{:S(2)}, u32[]{:S(2)}) %collective-permute-start) | collective-permute-done | bytes 2336 | tf_op jit(solution)/shard_map/ppermute | solution.py:91
  47.0 5.7 %collective-permute-done.1 = f32[96,6]{0,1:T(8,128)S(1)} collective-permute-done((f32[96,6]{0,1:T(8,128)S(1)}, f32[96,6]{0,1:T(8,128)S(1)}, u32[]{:S(2)}, u32[]{:S(2)}) %collective-permute-start.1) | collective-permute-done | bytes 2336 | tf_op jit(solution)/shard_map/ppermute | solution.py:91
  52.7 5.9 %collective-permute-done.2 = f32[96,6]{0,1:T(8,128)S(1)} collective-permute-done((f32[96,6]{0,1:T(8,128)S(1)}, f32[96,6]{0,1:T(8,128)S(1)}, u32[]{:S(2)}, u32[]{:S(2)}) %collective-permute-start.2) | collective-permute-done | bytes 2336 | tf_op jit(solution)/shard_map/ppermute | solution.py:91
  58.6 5.9 %collective-permute-done.3 = f32[96,6]{0,1:T(8,128)S(1)} collective-permute-done((f32[96,6]{0,1:T(8,128)S(1)}, f32[96,6]{0,1:T(8,128)S(1)}, u32[]{:S(2)}, u32[]{:S(2)}) %collective-permute-start.3) | collective-permute-done | bytes 2336 | tf_op jit(solution)/shard_map/ppermute | solution.py:91
  64.5 5.7 %collective-permute-done.4 = f32[96,6]{0,1:T(8,128)S(1)} collective-permute-done((f32[96,6]{0,1:T(8,128)S(1)}, f32[96,6]{0,1:T(8,128)S(1)}, u32[]{:S(2)}, u32[]{:S(2)}) %collective-permute-start.4) | collective-permute-done | bytes 2336 | tf_op jit(solution)/shard_map/ppermute | solution.py:91
  70.3 5.8 %collective-permute-done.5 = f32[96,6]{0,1:T(8,128)S(1)} collective-permute-done((f32[96,6]{0,1:T(8,128)S(1)}, f32[96,6]{0,1:T(8,128)S(1)}, u32[]{:S(2)}, u32[]{:S(2)}) %collective-permute-start.5) | collective-permute-done | bytes 2336 | tf_op jit(solution)/shard_map/ppermute | solution.py:91
  76.1 5.9 %collective-permute-done.6 = f32[96,6]{0,1:T(8,128)S(1)} collective-permute-done((f32[96,6]{0,1:T(8,128)S(1)}, f32[96,6]{0,1:T(8,128)S(1)}, u32[]{:S(2)}, u32[]{:S(2)}) %collective-permute-start.6) | collective-permute-done | bytes 2336 | tf_op jit(solution)/shard_map/ppermute | solution.py:91
  82.0 5.9 %collective-permute-done.7 = f32[96,6]{0,1:T(8,128)S(1)} collective-permute-done((f32[96,6]{0,1:T(8,128)S(1)}, f32[96,6]{0,1:T(8,128)S(1)}, u32[]{:S(2)}, u32[]{:S(2)}) %collective-permute-start.7) | collective-permute-done | bytes 2336 | tf_op jit(solution)/shard_map/ppermute | solution.py:91
  88.0 5.8 %collective-permute-done.8 = f32[96,6]{0,1:T(8,128)S(1)} collective-permute-done((f32[96,6]{0,1:T(8,128)S(1)}, f32[96,6]{0,1:T(8,128)S(1)}, u32[]{:S(2)}, u32[]{:S(2)}) %collective-permute-start.8) | collective-permute-done | bytes 2336 | tf_op jit(solution)/shard_map/ppermute | solution.py:91
  93.7 6.0 %collective-permute-done.9 = f32[96,6]{0,1:T(8,128)S(1)} collective-permute-done((f32[96,6]{0,1:T(8,128)S(1)}, f32[96,6]{0,1:T(8,128)S(1)}, u32[]{:S(2)}, u32[]{:S(2)}) %collective-permute-start.9) | collective-permute-done | bytes 2336 | tf_op jit(solution)/shard_map/ppermute | solution.py:91
  99.8 5.7 %collective-permute-done.10 = f32[96,6]{0,1:T(8,128)S(1)} collective-permute-done((f32[96,6]{0,1:T(8,128)S(1)}, f32[96,6]{0,1:T(8,128)S(1)}, u32[]{:S(2)}, u32[]{:S(2)}) %collective-permute-start.10) | collective-permute-done | bytes 2336 | tf_op jit(solution)/shard_map/ppermute | solution.py:91
  105.5 5.7 %collective-permute-done.11 = f32[96,6]{0,1:T(8,128)S(1)} collective-permute-done((f32[96,6]{0,1:T(8,128)S(1)}, f32[96,6]{0,1:T(8,128)S(1)}, u32[]{:S(2)}, u32[]{:S(2)}) %collective-permute-start.11) | collective-permute-done | bytes 2336 | tf_op jit(solution)/shard_map/ppermute | solution.py:91
  111.3 5.7 %collective-permute-done.12 = f32[96,6]{0,1:T(8,128)S(1)} collective-permute-done((f32[96,6]{0,1:T(8,128)S(1)}, f32[96,6]{0,1:T(8,128)S(1)}, u32[]{:S(2)}, u32[]{:S(2)}) %collective-permute-start.12) | collective-permute-done | bytes 2336 | tf_op jit(solution)/shard_map/ppermute | solution.py:91
  117.0 18.1 %all-gather = s32[16,96,6]{1,2,0:T(8,128)S(1)} all-gather(s32[1,96,6]{1,2,0:T(8,128)S(1)} %bitcast.62), channel_id=1, replica_groups=mesh['grp'=2,'ep'=16,'tp'=1] {'ep'}, dimensions={0}, use_global_device_ids=true | all-gather | bytes 39168 | tf_op jit(solution)/shard_map/all_gather | solution.py:86
  135.5 5.4 %collective-permute-done.14 = f32[96,6]{0,1:T(8,128)S(1)} collective-permute-done((f32[96,6]{0,1:T(8,128)S(1)}, f32[96,6]{0,1:T(8,128)S(1)}, u32[]{:S(2)}, u32[]{:S(2)}) %collective-permute-start.14) | collective-permute-done | bytes 2336 | tf_op jit(solution)/shard_map/ppermute | solution.py:91
  141.1 8.5 %fusion.12 = f32[1536,512]{1,0:T(8,128)} fusion(bf16[1536,2048]{1,0:T(8,128)(2,1)} %all-gather.3.cloned.1.call-done, bf16[1,2048,512]{2,1,0:T(8,128)(2,1)} %param.32), kind=kOutput, calls=%fused_computation.16 | convolution fusion | flops 3221225472 | bytes 11534336 | tf_op jit(solution)/shard_map/dot_general | solution.py:98
  149.6 11.8 %multiply_convert_fusion = bf16[1536,2048]{1,0:T(8,128)(2,1)} fusion(f32[1536]{0:T(1024)S(1)} %select_reduce_fusion, bf16[1,512,2048]{2,1,0:T(8,128)(2,1)S(1)} %copy-done, bf16[1536,2048]{1,0:T(8,128)(2,1)} %all-gather.3.cloned.1.call-done, f32[1536,512]{1,0:T(8,128)} %fusion.12, bf16[1,2048,512]{2,1,0:T(8,128)(2,1)} %param.33), kind=kOutput, calls=%fused_computation | convolution fusion | flops 6459752448 | bytes 19929088 | tf_op jit(solution)/shard_map/dot_general | solution.py:101
  169.5 3.4 %pad_maximum_fusion = f32[2,96,4096]{2,1,0:T(8,128)} fusion(f32[1,96,4096]{2,1,0:T(8,128)} %copy.56, f32[1,96,4096]{2,1,0:T(8,128)S(1)} %copy-done.4), kind=kLoop, calls=%fused_computation.3 | loop fusion | flops 786432 | bytes 6291456 | tf_op jit(solution)/shard_map/stack | solution.py:41
  172.9 71.8 %reduce-scatter.2.cloned.1.call-done = bf16[96,2048]{1,0:T(8,128)(2,1)} async-done(((bf16[1536,2048]{1,0:T(8,128)(2,1)}), bf16[96,2048]{1,0:T(8,128)(2,1)}) %reduce-scatter.2.cloned.1.call-update) | async-done | bytes 393232 | tf_op jit(solution)/shard_map/reduce_scatter | solution.py:104
  244.7 3.9 %fusion.3 = bf16[96,2048]{1,0:T(8,128)(2,1)} fusion(bf16[512,2048]{1,0:T(8,128)(2,1)} %param.37, bf16[96,2048]{1,0:T(8,128)(2,1)S(1)} %copy-done.5, bf16[2048,512]{1,0:T(8,128)(2,1)} %param.36, f32[96,2048]{1,0:T(8,128)S(1)} %get-tuple-element.11, bf16[96,2048]{1,0:T(8,128)(2,1)} %reduce-scatter.2.cloned.1.call-done, f32[96,512]{1,0:T(8,128)S(1)} %fusion.61), kind=kOutput, calls=%fused_computation.8 | convolution fusion | flops 404127744 | bytes 6356992 | tf_op jit(solution)/shard_map/dot_general | solution.py:142
  (69 shorter events, 25.9 us)
Async XLA Ops:
  7.2 142.5 %copy-start = (bf16[1,512,2048]{2,1,0:T(8,128)(2,1)S(1)}, bf16[1,512,2048]{2,1,0:T(8,128)(2,1)}, u32[]{:S(2)}) copy-start(bf16[1,512,2048]{2,1,0:T(8,128)(2,1)} %param.34) | copy-start | bytes 6291460
  7.2 133.9 %all-gather.3.cloned.1.call-start = ((), (), s32[]{:S(2)}) async-start(), calls=%async_computation.1 | async-start | bytes 6684672 | tf_op jit(solution)/shard_map/all_gather | solution.py:97
  25.3 5.8 %copy-start.7 = (f32[2,64,16,64]{3,2,1,0:T(8,128)S(1)}, f32[2,64,16,64]{3,2,1,0:T(8,128)}, u32[]{:S(2)}) copy-start(f32[2,64,16,64]{3,2,1,0:T(8,128)} %param.28) | copy-start | bytes 1572868
  31.0 3.9 %copy-start.1 = (f32[96,64,64]{0,2,1:T(8,128)}, f32[96,64,64]{0,2,1:T(8,128)S(1)}, u32[]{:S(2)}) copy-start(f32[96,64,64]{0,2,1:T(8,128)S(1)} %get-tuple-element.2) | copy-start | bytes 4718596
  31.0 3.9 %copy-start.2 = (f32[96,64,64]{0,2,1:T(8,128)}, f32[96,64,64]{0,2,1:T(8,128)S(1)}, u32[]{:S(2)}) copy-start(f32[96,64,64]{0,2,1:T(8,128)S(1)} %get-tuple-element.3) | copy-start | bytes 4718596
  35.8 3.4 %copy-start.11 = (f32[2048]{0:T(1024)S(1)}, f32[2048]{0:T(1024)}, u32[]{:S(2)}) copy-start(f32[2048]{0:T(1024)} %param.31) | copy-start | bytes 24580
  35.8 4.3 %copy-start.10 = (f32[96,6]{0,1:T(8,128)S(1)}, f32[96,6]{0,1:T(8,128)}, u32[]{:S(2)}) copy-start(f32[96,6]{0,1:T(8,128)} %param.39) | copy-start | bytes 6916
  35.8 81.1 %copy-start.12 = (s32[96,6]{0,1:T(8,128)S(1)}, s32[96,6]{0,1:T(8,128)}, u32[]{:S(2)}) copy-start(s32[96,6]{0,1:T(8,128)} %param.38) | copy-start | bytes 6916
  40.1 204.6 %reduce-scatter.2.cloned.1.call-start = ((), (), s32[]{:S(2)}) async-start(), calls=%async_computation.2 | async-start | bytes 6684672 | tf_op jit(solution)/shard_map/reduce_scatter | solution.py:104
  40.2 6.8 %collective-permute-start = (f32[96,6]{0,1:T(8,128)S(1)}, f32[96,6]{0,1:T(8,128)S(1)}, u32[]{:S(2)}, u32[]{:S(2)}) collective-permute-start(f32[96,6]{0,1:T(8,128)S(1)} %copy-done.10), channel_id=1, source_target_pairs={{0,1},{1,2},{2,3},{3,4},{4,5},{5,6},{6,7},{7,8},{8,9},{9,10},{10,1... | collective-permute-start | bytes 6920 | tf_op jit(solution)/shard_map/ppermute | solution.py:91
  47.0 5.7 %collective-permute-start.1 = (f32[96,6]{0,1:T(8,128)S(1)}, f32[96,6]{0,1:T(8,128)S(1)}, u32[]{:S(2)}, u32[]{:S(2)}) collective-permute-start(f32[96,6]{0,1:T(8,128)S(1)} %collective-permute-done), channel_id=1, source_target_pairs={{0,1},{1,2},{2,3},{3,4},{4,5},{5,6},{6,7},{7,8},{8,9},{9,10},{10,1... | collective-permute-start | bytes 6920 | tf_op jit(solution)/shard_map/ppermute | solution.py:91
  52.7 5.9 %collective-permute-start.2 = (f32[96,6]{0,1:T(8,128)S(1)}, f32[96,6]{0,1:T(8,128)S(1)}, u32[]{:S(2)}, u32[]{:S(2)}) collective-permute-start(f32[96,6]{0,1:T(8,128)S(1)} %collective-permute-done.1), channel_id=1, source_target_pairs={{0,1},{1,2},{2,3},{3,4},{4,5},{5,6},{6,7},{7,8},{8,9},{9,10},{10,1... | collective-permute-start | bytes 6920 | tf_op jit(solution)/shard_map/ppermute | solution.py:91
  58.6 5.9 %collective-permute-start.3 = (f32[96,6]{0,1:T(8,128)S(1)}, f32[96,6]{0,1:T(8,128)S(1)}, u32[]{:S(2)}, u32[]{:S(2)}) collective-permute-start(f32[96,6]{0,1:T(8,128)S(1)} %collective-permute-done.2), channel_id=1, source_target_pairs={{0,1},{1,2},{2,3},{3,4},{4,5},{5,6},{6,7},{7,8},{8,9},{9,10},{10,1... | collective-permute-start | bytes 6920 | tf_op jit(solution)/shard_map/ppermute | solution.py:91
  64.5 5.7 %collective-permute-start.4 = (f32[96,6]{0,1:T(8,128)S(1)}, f32[96,6]{0,1:T(8,128)S(1)}, u32[]{:S(2)}, u32[]{:S(2)}) collective-permute-start(f32[96,6]{0,1:T(8,128)S(1)} %collective-permute-done.3), channel_id=1, source_target_pairs={{0,1},{1,2},{2,3},{3,4},{4,5},{5,6},{6,7},{7,8},{8,9},{9,10},{10,1... | collective-permute-start | bytes 6920 | tf_op jit(solution)/shard_map/ppermute | solution.py:91
  70.2 5.8 %collective-permute-start.5 = (f32[96,6]{0,1:T(8,128)S(1)}, f32[96,6]{0,1:T(8,128)S(1)}, u32[]{:S(2)}, u32[]{:S(2)}) collective-permute-start(f32[96,6]{0,1:T(8,128)S(1)} %collective-permute-done.4), channel_id=1, source_target_pairs={{0,1},{1,2},{2,3},{3,4},{4,5},{5,6},{6,7},{7,8},{8,9},{9,10},{10,1... | collective-permute-start | bytes 6920 | tf_op jit(solution)/shard_map/ppermute | solution.py:91
  76.1 6.0 %collective-permute-start.6 = (f32[96,6]{0,1:T(8,128)S(1)}, f32[96,6]{0,1:T(8,128)S(1)}, u32[]{:S(2)}, u32[]{:S(2)}) collective-permute-start(f32[96,6]{0,1:T(8,128)S(1)} %collective-permute-done.5), channel_id=1, source_target_pairs={{0,1},{1,2},{2,3},{3,4},{4,5},{5,6},{6,7},{7,8},{8,9},{9,10},{10,1... | collective-permute-start | bytes 6920 | tf_op jit(solution)/shard_map/ppermute | solution.py:91
  82.0 6.0 %collective-permute-start.7 = (f32[96,6]{0,1:T(8,128)S(1)}, f32[96,6]{0,1:T(8,128)S(1)}, u32[]{:S(2)}, u32[]{:S(2)}) collective-permute-start(f32[96,6]{0,1:T(8,128)S(1)} %collective-permute-done.6), channel_id=1, source_target_pairs={{0,1},{1,2},{2,3},{3,4},{4,5},{5,6},{6,7},{7,8},{8,9},{9,10},{10,1... | collective-permute-start | bytes 6920 | tf_op jit(solution)/shard_map/ppermute | solution.py:91
  88.0 5.8 %collective-permute-start.8 = (f32[96,6]{0,1:T(8,128)S(1)}, f32[96,6]{0,1:T(8,128)S(1)}, u32[]{:S(2)}, u32[]{:S(2)}) collective-permute-start(f32[96,6]{0,1:T(8,128)S(1)} %collective-permute-done.7), channel_id=1, source_target_pairs={{0,1},{1,2},{2,3},{3,4},{4,5},{5,6},{6,7},{7,8},{8,9},{9,10},{10,1... | collective-permute-start | bytes 6920 | tf_op jit(solution)/shard_map/ppermute | solution.py:91
  93.7 6.0 %collective-permute-start.9 = (f32[96,6]{0,1:T(8,128)S(1)}, f32[96,6]{0,1:T(8,128)S(1)}, u32[]{:S(2)}, u32[]{:S(2)}) collective-permute-start(f32[96,6]{0,1:T(8,128)S(1)} %collective-permute-done.8), channel_id=1, source_target_pairs={{0,1},{1,2},{2,3},{3,4},{4,5},{5,6},{6,7},{7,8},{8,9},{9,10},{10,1... | collective-permute-start | bytes 6920 | tf_op jit(solution)/shard_map/ppermute | solution.py:91
  99.8 5.7 %collective-permute-start.10 = (f32[96,6]{0,1:T(8,128)S(1)}, f32[96,6]{0,1:T(8,128)S(1)}, u32[]{:S(2)}, u32[]{:S(2)}) collective-permute-start(f32[96,6]{0,1:T(8,128)S(1)} %collective-permute-done.9), channel_id=1, source_target_pairs={{0,1},{1,2},{2,3},{3,4},{4,5},{5,6},{6,7},{7,8},{8,9},{9,10},{10,1... | collective-permute-start | bytes 6920 | tf_op jit(solution)/shard_map/ppermute | solution.py:91
  105.5 5.7 %collective-permute-start.11 = (f32[96,6]{0,1:T(8,128)S(1)}, f32[96,6]{0,1:T(8,128)S(1)}, u32[]{:S(2)}, u32[]{:S(2)}) collective-permute-start(f32[96,6]{0,1:T(8,128)S(1)} %collective-permute-done.10), channel_id=1, source_target_pairs={{0,1},{1,2},{2,3},{3,4},{4,5},{5,6},{6,7},{7,8},{8,9},{9,10},{10,1... | collective-permute-start | bytes 6920 | tf_op jit(solution)/shard_map/ppermute | solution.py:91
  111.2 5.7 %collective-permute-start.12 = (f32[96,6]{0,1:T(8,128)S(1)}, f32[96,6]{0,1:T(8,128)S(1)}, u32[]{:S(2)}, u32[]{:S(2)}) collective-permute-start(f32[96,6]{0,1:T(8,128)S(1)} %collective-permute-done.11), channel_id=1, source_target_pairs={{0,1},{1,2},{2,3},{3,4},{4,5},{5,6},{6,7},{7,8},{8,9},{9,10},{10,1... | collective-permute-start | bytes 6920 | tf_op jit(solution)/shard_map/ppermute | solution.py:91
  117.0 18.2 %collective-permute-start.13 = (f32[96,6]{0,1:T(8,128)S(1)}, f32[96,6]{0,1:T(8,128)S(1)}, u32[]{:S(2)}, u32[]{:S(2)}) collective-permute-start(f32[96,6]{0,1:T(8,128)S(1)} %collective-permute-done.12), channel_id=1, source_target_pairs={{0,1},{1,2},{2,3},{3,4},{4,5},{5,6},{6,7},{7,8},{8,9},{9,10},{10,1... | collective-permute-start | bytes 6920 | tf_op jit(solution)/shard_map/ppermute | solution.py:91
  135.1 5.7 %collective-permute-start.14 = (f32[96,6]{0,1:T(8,128)S(1)}, f32[96,6]{0,1:T(8,128)S(1)}, u32[]{:S(2)}, u32[]{:S(2)}) collective-permute-start(f32[96,6]{0,1:T(8,128)S(1)} %collective-permute-done.13), channel_id=1, source_target_pairs={{0,1},{1,2},{2,3},{3,4},{4,5},{5,6},{6,7},{7,8},{8,9},{9,10},{10,1... | collective-permute-start | bytes 6920 | tf_op jit(solution)/shard_map/ppermute | solution.py:91
  (7 other events, 20.4 us)
Sparse Core Ops, SparseCore 0:
  40.2 64.3 all-gather.2
  161.5 83.0 reduce-scatter.1
